TPU v7x, 32 devices: a whole 2x2x4 slice. The times are simulated.
32 devices in a mesh: tp: 8 (over z, x), dp: 4 (over y, core).
Axes of the slice: x: 2, y: 2, z: 4, core: 2. Of those that a mesh axis runs over, the one named last changes fastest.
Arguments:
- tokens: bfloat16 [64, 4096], P('dp', 'tp'), may hold values from -6 to 6
- norm_gain: float32 [2, 4096], replicated, may hold values from 0.1 to 1.9
- w_in: bfloat16 [2, 4096, 2048], P(None, 'dp', 'tp'), may hold values from -0.09375 to 0.09375
- w_gate: bfloat16 [2, 4096, 2048], P(None, 'dp', 'tp'), may hold values from -0.1875 to 0.1875
- decay_rate: float32 [2, 128, 64], P(None, 'tp'), may hold values from 0.05 to 2
- frequency: float32 [2, 128, 64], P(None, 'tp'), may hold values from -3 to 3
- log_step: float32 [2, 128], P(None, 'tp'), may hold values from -3 to 0
- map_re: float32 [2, 128, 16, 64], P(None, 'tp'), may hold values from -1.5 to 1.5
- map_im: float32 [2, 128, 16, 64], P(None, 'tp'), may hold values from -1.5 to 1.5
- read_re: float32 [2, 128, 16, 64], P(None, 'tp'), may hold values from -0.5 to 0.5
- read_im: float32 [2, 128, 16, 64], P(None, 'tp'), may hold values from -0.5 to 0.5
- skip_weight: float32 [2, 128, 16], P(None, 'tp'), may hold values from -4 to 4
- w_out: bfloat16 [2, 2048, 4096], P(None, 'dp', 'tp'), may hold values from -0.25 to 0.25
- state_re: float32 [2, 64, 128, 64], P(None, 'dp', 'tp'), may hold values from -6 to 6
- state_im: float32 [2, 64, 128, 64], P(None, 'dp', 'tp'), may hold values from -6 to 6
Outputs:
- hidden: bfloat16 [64, 4096], P('dp', 'tp')
- new_re: float32 [2, 64, 128, 64], P(None, 'dp', 'tp')
- new_im: float32 [2, 64, 128, 64], P(None, 'dp', 'tp')
All inputs are finite; a program needn't handle non-finite values.
Results may differ from a plain program's by a relative error of at most 0.01.
Values may be sent and summed in bfloat16 or wider, within the bound.
A program may use at most 64 MiB of HBM per device.

v0:
```python
import jax
import jax.numpy as jnp
from jax import lax
from jax.sharding import PartitionSpec as P

EPSILON = 1e-06
HIGH = lax.Precision.HIGHEST


def state_update(
    inputs,
    old_re,
    old_im,
    decay_rate,
    frequency,
    log_step,
    map_re,
    map_im,
    read_re,
    read_im,
    skip_weight,
):
    lam_re = -decay_rate
    step_size = jnp.exp(log_step)[:, None]
    magnitude = jnp.exp(lam_re * step_size)
    decay_re = magnitude * jnp.cos(frequency * step_size)
    decay_im = magnitude * jnp.sin(frequency * step_size)
    modulus = lam_re * lam_re + frequency * frequency
    hold_re = ((decay_re - 1.0) * lam_re + decay_im * frequency) / modulus
    hold_im = (decay_im * lam_re - (decay_re - 1.0) * frequency) / modulus
    drive_re = hold_re[:, None, :] * map_re - hold_im[:, None, :] * map_im
    drive_im = hold_re[:, None, :] * map_im + hold_im[:, None, :] * map_re
    push_re = jnp.einsum("bgc,gcn->bgn", inputs, drive_re, precision=HIGH)
    push_im = jnp.einsum("bgc,gcn->bgn", inputs, drive_im, precision=HIGH)
    fresh_re = decay_re * old_re - decay_im * old_im + push_re
    fresh_im = decay_re * old_im + decay_im * old_re + push_im
    readout = (
        jnp.einsum("bgn,gcn->bgc", fresh_re, read_re, precision=HIGH)
        - jnp.einsum("bgn,gcn->bgc", fresh_im, read_im, precision=HIGH)
        + skip_weight * inputs
    )
    return (readout, fresh_re, fresh_im)


def local(
    tokens,
    norm_gain,
    w_in,
    w_gate,
    decay_rate,
    frequency,
    log_step,
    map_re,
    map_im,
    read_re,
    read_im,
    skip_weight,
    w_out,
    state_re,
    state_im,
):
    hidden = tokens
    seq_rows = tokens.shape[0]
    local_cols = w_in.shape[2]
    local_groups = decay_rate.shape[1]
    all_re = []
    all_im = []
    for layer in range(w_in.shape[0]):
        whole = lax.all_gather(hidden, "tp", axis=1, tiled=True)
        floats = whole.astype(jnp.float32)
        inv_scale = lax.rsqrt(jnp.mean(floats * floats, axis=-1, keepdims=True) + EPSILON)
        normed = (floats * inv_scale * norm_gain[layer]).astype(jnp.bfloat16)
        drive_sum = jnp.dot(
            normed,
            lax.all_gather(w_in[layer], "dp", axis=0, tiled=True),
            preferred_element_type=jnp.float32,
        )
        gate_sum = jnp.dot(
            normed,
            lax.all_gather(w_gate[layer], "dp", axis=0, tiled=True),
            preferred_element_type=jnp.float32,
        )
        projected = drive_sum.astype(jnp.bfloat16)
        gate = gate_sum.astype(jnp.bfloat16)
        inputs = projected.astype(jnp.float32).reshape(seq_rows, local_groups, -1)
        readout, fresh_re, fresh_im = state_update(
            inputs,
            state_re[layer],
            state_im[layer],
            decay_rate[layer],
            frequency[layer],
            log_step[layer],
            map_re[layer],
            map_im[layer],
            read_re[layer],
            read_im[layer],
            skip_weight[layer],
        )
        activated = jax.nn.gelu(readout.reshape(seq_rows, local_cols))
        mixer = (activated * jax.nn.sigmoid(gate.astype(jnp.float32))).astype(jnp.bfloat16)
        full_rows = lax.all_gather(mixer, "tp", axis=1, tiled=True)
        mixed = jnp.dot(
            full_rows,
            lax.all_gather(w_out[layer], "dp", axis=0, tiled=True),
            preferred_element_type=jnp.float32,
        )
        hidden = (hidden.astype(jnp.float32) + mixed).astype(jnp.bfloat16)
        all_re.append(fresh_re)
        all_im.append(fresh_im)
    return (hidden, jnp.stack(all_re), jnp.stack(all_im))


def solution(mesh):
    return jax.shard_map(
        local,
        mesh=mesh,
        in_specs=(
            P("dp", "tp"),
            P(),
            P(None, "dp", "tp"),
            P(None, "dp", "tp"),
            P(None, "tp", None),
            P(None, "tp", None),
            P(None, "tp"),
            P(None, "tp", None, None),
            P(None, "tp", None, None),
            P(None, "tp", None, None),
            P(None, "tp", None, None),
            P(None, "tp", None),
            P(None, "dp", "tp"),
            P(None, "dp", "tp", None),
            P(None, "dp", "tp", None),
        ),
        out_specs=(P("dp", "tp"), P(None, "dp", "tp", None), P(None, "dp", "tp", None)),
        check_vma=False,
    )
```

profile of v0, /device:TPU:0, one launch (start us, length us, event | category | flops | bytes accessed | tf_op | source)
XLA Modules:
  0.0 173.4 jit_solution(2117782072541456028)
XLA Ops:
  7.2 0.0 copy-start
  7.2 0.0 all-gather.13.cloned.1.call-start
  7.2 2.4 %fusion.159 = (bf16[1,1024,256]{2,1,0:T(8,128)(2,1)}, bf16[1,1024,256]{2,1,0:T(8,128)(2,1)}) fusion(bf16[2,1024,256]{2,1,0:T(8,128)(2,1)} %param.17), kind=kLoop, calls=%fused_computation.165 | loop fusion | bytes 2097152 | tf_op jit(solution)/shard_map/slice | solution.py:75
  9.6 0.0 all-gather.13.cloned.1.call-update
  9.6 0.0 all-gather.15.cloned.1.call-start
  9.6 0.0 copy-done
  9.7 1.1 fusion.160
  10.7 0.0 all-gather.15.cloned.1.call-update
  10.7 0.0 copy-start.13
  10.7 0.0 copy-start.9
  10.8 0.0 copy-start.10
  10.8 0.0 copy-start.8
  10.8 0.0 copy-start.11
  10.8 0.0 copy-start.12
  10.8 0.0 copy-start.5
  10.8 0.0 copy-start.6
  10.8 0.0 all-gather.17.cloned.1.call-start
  10.9 0.3 copy-done.1
  11.2 1.0 fusion.158
  12.2 0.0 all-gather.17.cloned.1.call-update
  12.2 0.0 all-gather.19.cloned.1.call-start
  12.3 0.5 all-gather.19.cloned.1.call-update
  12.8 0.0 all-gather.21.cloned.1.call-start
  12.8 0.5 all-gather.21.cloned.1.call-update
  13.4 0.0 all-gather.23.cloned.1.call-start
  13.4 0.0 copy-start.2
  13.4 0.0 copy-start.3
  13.4 0.5 all-gather.23.cloned.1.call-update
  14.0 0.1 multiply_bitcast_fusion.1
  14.1 0.2 fusion.149
  14.3 32.3 %all_gather.30 = bf16[16,4096]{1,0:T(8,128)(2,1)S(1)} all-gather(bf16[16,512]{1,0:T(8,128)(2,1)S(1)} %copy-done.8), channel_id=1, replica_groups=mesh['tp'=8,'dp'=4] {'tp'}, dimensions={1}, use_global_device_ids=true | all-gather | bytes 147456 | tf_op jit(solution)/shard_map/all_gather | solution.py:69
  46.7 0.1 fusion.86
  46.9 0.0 copy-done.12
  46.9 0.0 copy-done.5
  46.9 0.0 copy-start.4
  46.9 0.0 all-gather.13.cloned.1.call-done
  47.0 0.0 copy-start.7
  47.0 2.1 %fusion.32 = bf16[16,256]{1,0:T(8,128)(2,1)S(1)} fusion(bf16[1,4096,256]{2,1,0:T(8,128)(2,1)} %all-gather.13.cloned.1.call-done, bf16[16,4096]{1,0:T(8,128)(2,1)S(1)} %all_gather.30, f32[4096]{0:T(1024)S(1)} %bitcast.306, f32[16]{0:T(128)S(1)} %add_rsqrt_fusion.1), kind=kOutput, calls=%fused_computation.30 | convolution fusion | flops 33820672 | bytes 2252864 | tf_op jit(solution)/shard_map/dot_general | solution.py:73
  49.1 0.1 reshape.300
  49.2 0.2 fusion.15
  49.4 0.2 fusion.14
  49.6 0.3 fusion.100
  50.0 0.3 fusion.19
  50.4 0.1 reshape.302
  50.5 8.7 %all-gather.15.cloned.1.call-done = bf16[1,4096,256]{2,1,0:T(8,128)(2,1)} async-done(((bf16[1,1024,256]{2,1,0:T(8,128)(2,1)}), bf16[1,4096,256]{2,1,0:T(8,128)(2,1)}) %all-gather.15.cloned.1.call-update) | async-done | bytes 2097168 | tf_op jit(solution)/shard_map/all_gather | solution.py:80
  59.2 2.0 %fusion.56 = bf16[16,256]{1,0:T(8,128)(2,1)S(1)} fusion(bf16[1,4096,256]{2,1,0:T(8,128)(2,1)} %all-gather.15.cloned.1.call-done, bf16[16,4096]{1,0:T(8,128)(2,1)S(1)} %all_gather.30, f32[4096]{0:T(1024)S(1)} %bitcast.307, f32[16]{0:T(128)S(1)} %add_rsqrt_fusion.1, f32[16,256]{1,0:T(8,128)S(1)} %reshape.302), kind=kOutput, calls=%fused_computation.38 | convolution fusion | flops 33878016 | bytes 2269248 | tf_op jit(solution)/shard_map/dot_general | solution.py:78
  61.2 30.6 %all_gather.33 = bf16[16,2048]{1,0:T(8,128)(2,1)S(1)} all-gather(bf16[16,256]{1,0:T(8,128)(2,1)S(1)} %fusion.56), channel_id=1, replica_groups=mesh['tp'=8,'dp'=4] {'tp'}, dimensions={1}, use_global_device_ids=true | all-gather | bytes 73728 | tf_op jit(solution)/shard_map/all_gather | solution.py:101
  91.8 2.3 %fusion.29 = bf16[16,512]{1,0:T(8,128)(2,1)S(1)} fusion(bf16[16,2048]{1,0:T(8,128)(2,1)S(1)} %all_gather.33, bf16[1,2048,512]{2,1,0:T(8,128)(2,1)} %all-gather.17.cloned.1.call-done, bf16[16,512]{1,0:T(8,128)(2,1)S(1)} %copy-done.8), kind=kOutput, calls=%fused_computation.29 | convolution fusion | flops 33579008 | bytes 2195456 | tf_op jit(solution)/shard_map/dot_general | solution.py:102
  94.1 30.5 %all_gather.35 = bf16[16,4096]{1,0:T(8,128)(2,1)S(1)} all-gather(bf16[16,512]{1,0:T(8,128)(2,1)S(1)} %fusion.29), channel_id=1, replica_groups=mesh['tp'=8,'dp'=4] {'tp'}, dimensions={1}, use_global_device_ids=true | all-gather | bytes 147456 | tf_op jit(solution)/shard_map/all_gather | solution.py:69
  124.6 0.1 fusion.89
  124.8 0.0 all-gather.19.cloned.1.call-done
  124.8 2.0 %fusion.59 = bf16[16,256]{1,0:T(8,128)(2,1)S(1)} fusion(bf16[1,4096,256]{2,1,0:T(8,128)(2,1)} %all-gather.19.cloned.1.call-done, bf16[16,4096]{1,0:T(8,128)(2,1)S(1)} %all_gather.35, f32[4096]{0:T(1024)S(1)} %bitcast.304, f32[16]{0:T(128)S(1)} %add_rsqrt_fusion), kind=kOutput, calls=%fused_computation.39 | convolution fusion | flops 33820672 | bytes 2252864 | tf_op jit(solution)/shard_map/dot_general | solution.py:73
  126.9 0.1 reshape.303
  127.0 0.2 fusion.12
  127.2 0.8 copy.43
  128.0 0.2 fusion.13
  128.3 0.8 copy.42
  129.1 0.3 fusion.93
  129.4 0.3 fusion.17
  129.8 0.1 reshape.305
  129.9 1.5 all-gather.21.cloned.1.call-done
  131.4 2.0 %fusion.83 = bf16[16,256]{1,0:T(8,128)(2,1)S(1)} fusion(bf16[1,4096,256]{2,1,0:T(8,128)(2,1)} %all-gather.21.cloned.1.call-done, bf16[16,4096]{1,0:T(8,128)(2,1)S(1)} %all_gather.35, f32[4096]{0:T(1024)S(1)} %bitcast.305, f32[16]{0:T(128)S(1)} %add_rsqrt_fusion, f32[16,256]{1,0:T(8,128)S(1)} %reshape.305), kind=kOutput, calls=%fused_computation.47 | convolution fusion | flops 33878016 | bytes 2269248 | tf_op jit(solution)/shard_map/dot_general | solution.py:78
  133.4 30.6 %all_gather.38 = bf16[16,2048]{1,0:T(8,128)(2,1)S(1)} all-gather(bf16[16,256]{1,0:T(8,128)(2,1)S(1)} %fusion.83), channel_id=1, replica_groups=mesh['tp'=8,'dp'=4] {'tp'}, dimensions={1}, use_global_device_ids=true | all-gather | bytes 73728 | tf_op jit(solution)/shard_map/all_gather | solution.py:101
  164.0 2.6 %fusion.26 = bf16[16,512]{1,0:T(8,128)(2,1)} fusion(bf16[16,2048]{1,0:T(8,128)(2,1)S(1)} %all_gather.38, bf16[1,2048,512]{2,1,0:T(8,128)(2,1)} %all-gather.23.cloned.1.call-done, bf16[16,512]{1,0:T(8,128)(2,1)S(1)} %fusion.29), kind=kOutput, calls=%fused_computation.28 | convolution fusion | flops 33579008 | bytes 2195456 | tf_op jit(solution)/shard_map/dot_general | solution.py:102
  (23 shorter events, 0.3 us)
Async XLA Ops:
  7.2 2.5 %copy-start = (bf16[2,1024,256]{2,1,0:T(8,128)(2,1)S(1)}, bf16[2,1024,256]{2,1,0:T(8,128)(2,1)}, u32[]{:S(2)}) copy-start(bf16[2,1024,256]{2,1,0:T(8,128)(2,1)} %param.18) | copy-start | bytes 3145732
  7.2 39.8 %all-gather.13.cloned.1.call-start = ((), (), s32[]{:S(2)}) async-start(), calls=%async_computation | async-start | bytes 2621440 | tf_op jit(solution)/shard_map/all_gather | solution.py:75
  9.6 1.6 copy-start.1
  9.6 49.6 %all-gather.15.cloned.1.call-start = ((), (), s32[]{:S(2)}) async-start(), calls=%async_computation.1 | async-start | bytes 2621440 | tf_op jit(solution)/shard_map/all_gather | solution.py:80
  10.7 3.2 %copy-start.13 = (f32[2,16]{1,0:T(2,128)S(1)}, f32[2,16]{1,0:T(2,128)}, u32[]{:S(2)}) copy-start(f32[2,16]{1,0:T(2,128)} %param.21) | copy-start | bytes 388
  10.7 3.2 %copy-start.9 = (f32[2,16,64]{2,1,0:T(8,128)S(1)}, f32[2,16,64]{2,1,0:T(8,128)}, u32[]{:S(2)}) copy-start(f32[2,16,64]{2,1,0:T(8,128)} %param.19) | copy-start | bytes 24580
  10.8 3.2 %copy-start.10 = (f32[2,16,64]{2,1,0:T(8,128)S(1)}, f32[2,16,64]{2,1,0:T(8,128)}, u32[]{:S(2)}) copy-start(f32[2,16,64]{2,1,0:T(8,128)} %param.20) | copy-start | bytes 24580
  10.8 3.5 %copy-start.8 = (bf16[16,512]{1,0:T(8,128)(2,1)S(1)}, bf16[16,512]{1,0:T(8,128)(2,1)}, u32[]{:S(2)}) copy-start(bf16[16,512]{1,0:T(8,128)(2,1)} %param.15) | copy-start | bytes 49156
  10.8 36.0 %copy-start.11 = (f32[2,4096]{1,0:T(2,128)S(1)}, f32[2,4096]{1,0:T(2,128)}, u32[]{:S(2)}) copy-start(f32[2,4096]{1,0:T(2,128)} %param.16) | copy-start | bytes 98308
  10.8 36.1 %copy-start.12 = (f32[2,16,16]{2,1,0:T(8,128)S(1)}, f32[2,16,16]{2,1,0:T(8,128)}, u32[]{:S(2)}) copy-start(f32[2,16,16]{2,1,0:T(8,128)} %param.26) | copy-start | bytes 6148
  10.8 36.1 %copy-start.5 = (f32[2,16,16,64]{3,2,1,0:T(8,128)S(1)}, f32[2,16,16,64]{3,2,1,0:T(8,128)}, u32[]{:S(2)}) copy-start(f32[2,16,16,64]{3,2,1,0:T(8,128)} %param.29) | copy-start | bytes 393220
  10.8 36.1 %copy-start.6 = (f32[2,16,16,64]{3,2,1,0:T(8,128)S(1)}, f32[2,16,16,64]{3,2,1,0:T(8,128)}, u32[]{:S(2)}) copy-start(f32[2,16,16,64]{3,2,1,0:T(8,128)} %param.28) | copy-start | bytes 393220
  10.8 81.0 %all-gather.17.cloned.1.call-start = ((), (), s32[]{:S(2)}) async-start(), calls=%async_computation.2 | async-start | bytes 2621440 | tf_op jit(solution)/shard_map/all_gather | solution.py:104
  12.2 112.6 %all-gather.19.cloned.1.call-start = ((), (), s32[]{:S(2)}) async-start(), calls=%async_computation.3 | async-start | bytes 2621440 | tf_op jit(solution)/shard_map/all_gather | solution.py:75
  12.8 118.6 %all-gather.21.cloned.1.call-start = ((), (), s32[]{:S(2)}) async-start(), calls=%async_computation.4 | async-start | bytes 2621440 | tf_op jit(solution)/shard_map/all_gather | solution.py:80
  13.4 150.6 %all-gather.23.cloned.1.call-start = ((), (), s32[]{:S(2)}) async-start(), calls=%async_computation.5 | async-start | bytes 2621440 | tf_op jit(solution)/shard_map/all_gather | solution.py:104
  13.4 35.7 %copy-start.2 = (f32[2,16,16,64]{3,2,1,0:T(8,128)S(1)}, f32[2,16,16,64]{3,2,1,0:T(8,128)}, u32[]{:S(2)}) copy-start(f32[2,16,16,64]{3,2,1,0:T(8,128)} %param.23) | copy-start | bytes 393220
  13.4 35.7 %copy-start.3 = (f32[2,16,16,64]{3,2,1,0:T(8,128)S(1)}, f32[2,16,16,64]{3,2,1,0:T(8,128)}, u32[]{:S(2)}) copy-start(f32[2,16,16,64]{3,2,1,0:T(8,128)} %param.22) | copy-start | bytes 393220
  46.9 2.7 %copy-start.4 = (f32[2,16,16,64]{3,2,1,0:T(8,128)S(1)}, f32[2,16,16,64]{3,2,1,0:T(8,128)}, u32[]{:S(2)}) copy-start(f32[2,16,16,64]{3,2,1,0:T(8,128)} %param.24) | copy-start | bytes 393220
  47.0 3.0 %copy-start.7 = (f32[2,16,16,64]{3,2,1,0:T(8,128)S(1)}, f32[2,16,16,64]{3,2,1,0:T(8,128)}, u32[]{:S(2)}) copy-start(f32[2,16,16,64]{3,2,1,0:T(8,128)} %param.25) | copy-start | bytes 393220
Sparse Core Ops, SparseCore 0:
  9.7 25.2 all-gather.12
  36.6 22.5 all-gather.14
  60.8 22.5 all-gather.16
  84.8 22.5 all-gather.18
  108.8 22.5 all-gather.20
  132.8 22.5 all-gather.22
where the time goes:
time: 174 us; the launch traced here: 173 us
  blocking collectives  124 us (71%)
  matrix products  15.2 us (9%)
  between operations  14.5 us (8%)
  waiting for transfers between devices  11.8 us (7%)
  local copies, waits for them, and re-layouts  6.96 us (4%)
    all_gather x2, blocking collectives, local(): whole = lax.all_gather(hidden, 'tp', axis=1, tiled=True)  62.9 us
    all_gather x2, blocking collectives, local(): full_rows = lax.all_gather(mixer, 'tp', axis=1, tiled=True)  61.2 us
    all_gather x2, waiting for transfers between devices, local(): lax.all_gather(w_gate[layer], 'dp', axis=0, tiled=True)  10.2 us
    dot_general x2, matrix products, local(): jnp.dot(full_rows, lax.all_gather(w_out[layer], 'dp', axis=0, tiled=True)...  4.87 us
    dot_general x2, matrix products, local(): jnp.dot(normed, lax.all_gather(w_in[layer], 'dp', axis=0, tiled=True), pr...  4.09 us
    dot_general x2, matrix products, local(): jnp.dot(normed, lax.all_gather(w_gate[layer], 'dp', axis=0, tiled=True),...  4.04 us
  transfers between devices with their start and end apart: 6, of which 2 were waited for; matrix products, arithmetic and copies ran while one was open for 10% of the time, Pallas kernels for 0%

commit v1 on v0

v1 whole, which is shorter than its diff:
```python
import functools

import jax
import jax.numpy as jnp
from jax import lax
from jax.experimental import pallas as pl
from jax.experimental.pallas import tpu as pltpu
from jax.sharding import PartitionSpec as P

EPSILON = 1e-06
F32 = jnp.float32
BF16 = jnp.bfloat16
TAIL = 128


def dot(a, b):
    return jnp.dot(a, b, preferred_element_type=F32)


def dot_t(a, b):
    return lax.dot_general(a, b, (((1,), (1,)), ((), ())), preferred_element_type=F32)


def kernel(
    tp_size,
    dp_size,
    bundle,
    tokens,
    gain,
    w_in,
    w_gate,
    rate,
    freq,
    log_step,
    map_re,
    map_im,
    read_re,
    read_im,
    skip,
    w_out,
    state_re,
    state_im,
    hidden_out,
    new_re,
    new_im,
    tok,
    gain_v,
    win_v,
    wgate_v,
    rate_v,
    freq_v,
    step_v,
    mapre_v,
    mapim_v,
    readre_v,
    readim_v,
    skip_v,
    wout_v,
    stre_v,
    stim_v,
    nre_v,
    nim_v,
    drive,
    read,
    held,
    skip_flat,
    xbuf,
    sbuf,
    rbuf,
    mix,
    mbuf,
    obuf,
    orbuf,
    hid,
    load_sem,
    a_send,
    a_recv,
    b_send,
    b_recv,
    c_send,
    c_recv,
    d_send,
    d_recv,
    out_sem,
):
    j = lax.axis_index("tp")
    i = lax.axis_index("dp")
    per = tp_size // dp_size
    layers, groups, states = rate.shape
    channels = skip.shape[2]
    seqs, feats = tokens.shape
    cols = w_in.shape[2]
    depth = w_in.shape[1]
    total_feats = gain.shape[1]
    bundles = groups // bundle
    bc, bn = bundle * channels, bundle * states
    target = lax.div(j, per)
    slot = lax.rem(j, per)
    is_self = target == i

    gain_cols = pl.ds(pl.multiple_of(i * depth, depth), depth)
    loads = [
        (tokens, tok),
        (rate, rate_v),
        (freq, freq_v),
        (log_step, step_v),
        (map_re, mapre_v),
        (map_im, mapim_v),
        (state_re, stre_v),
        (state_im, stim_v),
        (read_re, readre_v),
        (read_im, readim_v),
        (skip, skip_v),
        (gain.at[:, gain_cols], gain_v),
        (w_in, win_v),
        (w_gate, wgate_v),
        (w_out, wout_v),
    ]
    copies = [
        pltpu.make_async_copy(src, dst, load_sem.at[k]) for k, (src, dst) in enumerate(loads)
    ]
    for copy in copies:
        copy.start()

    barrier = pltpu.get_barrier_semaphore()
    for t in range(per):
        for d in range(dp_size):
            src_tp = i * per + t

            @pl.when(jnp.logical_or(src_tp != j, i != d))
            def _():
                pl.semaphore_signal(barrier, inc=1, device_id={"tp": src_tp, "dp": jnp.int32(d)})

    for r in range(1, dp_size):
        pl.semaphore_signal(
            barrier, inc=1, device_id={"tp": j, "dp": lax.rem(i + r, dp_size)}
        )

    pending = []
    order = sorted(range(tp_size), key=lambda r: -min(r, tp_size - r))

    def spread(src, buf, send, recv, layer):
        dst = buf.at[layer, slot, i]
        for r in order:
            copy = pltpu.make_async_remote_copy(
                src_ref=src,
                dst_ref=dst,
                send_sem=send.at[layer, r],
                recv_sem=recv.at[layer, slot, i],
                device_id={"tp": lax.rem(j + r, tp_size), "dp": target},
            )
            if r:
                copy.start()
                pending.append((False, copy))
            else:
                own = pltpu.make_async_copy(src, dst, recv.at[layer, slot, i])

                @pl.when(is_self)
                def _():
                    own.start()

                @pl.when(jnp.logical_not(is_self))
                def _():
                    copy.start()

                pending.append((True, copy))

    def gather_wait(buf, recv, layer):
        for t in range(per):
            for d in range(dp_size):
                ref = buf.at[layer, t, d]
                pltpu.make_async_copy(ref, ref, recv.at[layer, t, d]).wait()

    def scatter(src, dst, send, recv, layer):
        for r in range(dp_size - 1, 0, -1):
            d = lax.rem(i + r, dp_size)
            copy = pltpu.make_async_remote_copy(
                src_ref=src.at[layer, d],
                dst_ref=dst.at[layer, i],
                send_sem=send.at[layer, r],
                recv_sem=recv.at[layer, i],
                device_id={"tp": j, "dp": d},
            )
            copy.start()
            pending.append((False, copy))

    def collect(src, dst, recv, layer):
        acc = src[layer, i].astype(F32)
        for r in range(1, dp_size):
            d = lax.rem(i + r, dp_size)
            ref = dst.at[layer, d]
            pltpu.make_async_copy(ref, ref, recv.at[layer, d]).wait()
            acc = acc + dst[layer, d].astype(F32)
        return acc

    def prepare(layer):
        lam_re = -rate_v[layer]
        lam_im = freq_v[layer]
        eye = lax.broadcasted_iota(jnp.int32, (groups, groups), 0) == lax.broadcasted_iota(
            jnp.int32, (groups, groups), 1
        )
        log_col = jnp.sum(
            jnp.where(eye, step_v[layer : layer + 1, :], 0.0), axis=1, keepdims=True
        )
        step_size = jnp.exp(log_col)
        magnitude = jnp.exp(lam_re * step_size)
        decay_re = magnitude * jnp.cos(lam_im * step_size)
        decay_im = magnitude * jnp.sin(lam_im * step_size)
        modulus = lam_re * lam_re + lam_im * lam_im
        hold_re = ((decay_re - 1.0) * lam_re + decay_im * lam_im) / modulus
        hold_im = (decay_im * lam_re - (decay_re - 1.0) * lam_im) / modulus
        for g in range(groups):
            q, k = g // bundle, g % bundle
            rows = slice(g * channels, (g + 1) * channels)
            to = slice(k * channels, (k + 1) * channels)
            lanes = slice(k * states, (k + 1) * states)
            lanes_im = slice(bn + k * states, bn + (k + 1) * states)
            hr, hi = hold_re[g : g + 1, :], hold_im[g : g + 1, :]
            mr, mi = mapre_v[layer, rows, :], mapim_v[layer, rows, :]
            drive[layer, q, to, lanes] = (hr * mr - hi * mi).astype(BF16)
            drive[layer, q, to, lanes_im] = (hr * mi + hi * mr).astype(BF16)
            read[layer, q, to, lanes] = readre_v[layer, rows, :].astype(BF16)
            read[layer, q, to, lanes_im] = (-readim_v[layer, rows, :]).astype(BF16)
            where = pl.ds(layer * seqs * groups + g, seqs, stride=groups)
            old_re, old_im = stre_v[where, :], stim_v[where, :]
            dr, di = decay_re[g : g + 1, :], decay_im[g : g + 1, :]
            held[layer, q, :, lanes] = dr * old_re - di * old_im
            held[layer, q, :, lanes_im] = dr * old_im + di * old_re
            skip_flat[layer, 0:1, g * channels : (g + 1) * channels] = skip_v[
                layer, g : g + 1, :
            ]

    drive[...] = jnp.zeros_like(drive)
    read[...] = jnp.zeros_like(read)
    copies[0].wait()
    pl.semaphore_wait(barrier, tp_size - is_self.astype(jnp.int32) + dp_size - 1)
    spread(tok, xbuf, a_send, a_recv, 0)
    for copy in copies[1:11]:
        copy.wait()
    for layer in range(layers):
        prepare(layer)
    for copy in copies[11:]:
        copy.wait()

    out_copies = []
    rows_all = dp_size * seqs
    residual = tok[...].astype(F32)
    for layer in range(layers):
        gather_wait(xbuf, a_recv, layer)
        squares = jnp.zeros((rows_all, 1), F32)
        drive_sum = jnp.zeros((rows_all, cols), F32)
        gate_sum = jnp.zeros((rows_all, cols), F32)
        for t in range(per):
            part = slice(t * feats, (t + 1) * feats)
            x = xbuf[layer, t].reshape(rows_all, feats).astype(F32)
            squares = squares + jnp.sum(x * x, axis=1, keepdims=True)
            scaled = (x * gain_v[layer : layer + 1, part]).astype(BF16)
            drive_sum = drive_sum + dot(scaled, win_v[layer, part, :])
            gate_sum = gate_sum + dot(scaled, wgate_v[layer, part, :])
        high = squares.astype(BF16).astype(F32)
        lane = lax.broadcasted_iota(jnp.int32, (rows_all, TAIL), 1)
        tail = jnp.where(lane < TAIL // 2, high, squares - high).astype(BF16)
        sbuf[layer, :, :, 0:TAIL] = tail.reshape(dp_size, seqs, TAIL)
        sbuf[layer, :, :, TAIL : TAIL + cols] = drive_sum.astype(BF16).reshape(
            dp_size, seqs, cols
        )
        sbuf[layer, :, :, TAIL + cols :] = gate_sum.astype(BF16).reshape(dp_size, seqs, cols)
        scatter(sbuf, rbuf, b_send, b_recv, layer)
        acc = collect(sbuf, rbuf, b_recv, layer)
        mean = (acc[:, 0:1] + acc[:, TAIL // 2 : TAIL // 2 + 1]) * (1.0 / total_feats)
        inv_scale = lax.rsqrt(mean + EPSILON)
        projected = (acc[:, TAIL : TAIL + cols] * inv_scale).astype(BF16)
        gate = (acc[:, TAIL + cols :] * inv_scale).astype(BF16).astype(F32)
        fresh = []
        for q in range(bundles):
            part = slice(q * bc, (q + 1) * bc)
            u = projected[:, part]
            new = held[layer, q] + dot(u, drive[layer, q])
            fresh.append(new)
            readout = dot_t(new.astype(BF16), read[layer, q])
            readout = readout + skip_flat[layer, 0:1, part] * u.astype(F32)
            inner = 0.7978845608028654 * (readout + 0.044715 * readout * readout * readout)
            activated = 0.5 * readout * (1.0 + jnp.tanh(inner))
            opened = 0.5 * (jnp.tanh(0.5 * gate[:, part]) + 1.0)
            mix[layer, :, part] = (activated * opened).astype(BF16)
        spread(mix.at[layer], mbuf, c_send, c_recv, layer)
        for g in range(groups):
            q, k = g // bundle, g % bundle
            where = pl.ds(layer * seqs * groups + g, seqs, stride=groups)
            nre_v[where, :] = fresh[q][:, k * states : (k + 1) * states]
            nim_v[where, :] = fresh[q][:, bn + k * states : bn + (k + 1) * states]
        block = pl.ds(layer * seqs * groups, seqs * groups)
        for k, (src, dst) in enumerate(((nre_v, new_re), (nim_v, new_im))):
            copy = pltpu.make_async_copy(src.at[block], dst.at[block], out_sem.at[layer, k])
            copy.start()
            out_copies.append(copy)
        gather_wait(mbuf, c_recv, layer)
        mixed = jnp.zeros((rows_all, feats), F32)
        for t in range(per):
            part = slice(t * cols, (t + 1) * cols)
            mixed = mixed + dot(mbuf[layer, t].reshape(rows_all, cols), wout_v[layer, part, :])
        obuf[layer] = mixed.astype(BF16).reshape(dp_size, seqs, feats)
        scatter(obuf, orbuf, d_send, d_recv, layer)
        hidden = (residual + collect(obuf, orbuf, d_recv, layer)).astype(BF16)
        if layer + 1 < layers:
            hid[layer] = hidden
            spread(hid.at[layer], xbuf, a_send, a_recv, layer + 1)
            residual = hidden.astype(F32)
        else:
            hidden_out[...] = hidden
    for conditional, copy in pending:
        if conditional:

            @pl.when(jnp.logical_not(is_self))
            def _():
                copy.wait_send()
        else:
            copy.wait_send()
    for copy in out_copies:
        copy.wait()


def local(tp_size, dp_size, *args):
    (tokens, gain, w_in, w_gate, rate, freq, log_step, map_re, map_im, read_re, read_im) = args[:11]
    skip, w_out, state_re, state_im = args[11:]
    layers, groups, channels, states = map_re.shape
    seqs, feats = tokens.shape
    depth, cols = w_in.shape[1:]
    per = tp_size // dp_size
    bundle = min(groups, max(1, 128 // channels))
    bundles = groups // bundle
    bc, bn = bundle * channels, bundle * states
    flat = lambda a: a.reshape(layers, groups * channels, states)
    rows = lambda a: a.reshape(layers * seqs * groups, states)
    width = TAIL + 2 * cols
    vm = pltpu.VMEM
    dma = pltpu.SemaphoreType.DMA
    scratch = [
        vm((seqs, feats), BF16),
        vm((layers, depth), F32),
        vm(w_in.shape, BF16),
        vm(w_gate.shape, BF16),
        vm(rate.shape, F32),
        vm(freq.shape, F32),
        vm(log_step.shape, F32),
        vm((layers, groups * channels, states), F32),
        vm((layers, groups * channels, states), F32),
        vm((layers, groups * channels, states), F32),
        vm((layers, groups * channels, states), F32),
        vm(skip.shape, F32),
        vm(w_out.shape, BF16),
        vm((layers * seqs * groups, states), F32),
        vm((layers * seqs * groups, states), F32),
        vm((layers * seqs * groups, states), F32),
        vm((layers * seqs * groups, states), F32),
        vm((layers, bundles, bc, 2 * bn), BF16),
        vm((layers, bundles, bc, 2 * bn), BF16),
        vm((layers, bundles, seqs, 2 * bn), F32),
        vm((layers, 8, cols), F32),
        vm((layers, per, dp_size, seqs, feats), BF16),
        vm((layers, dp_size, seqs, width), BF16),
        vm((layers, dp_size, seqs, width), BF16),
        vm((layers, seqs, cols), BF16),
        vm((layers, per, dp_size, seqs, cols), BF16),
        vm((layers, dp_size, seqs, feats), BF16),
        vm((layers, dp_size, seqs, feats), BF16),
        vm((layers, seqs, feats), BF16),
        dma((15,)),
        dma((layers, tp_size)),
        dma((layers, per, dp_size)),
        dma((layers, dp_size)),
        dma((layers, dp_size)),
        dma((layers, tp_size)),
        dma((layers, per, dp_size)),
        dma((layers, dp_size)),
        dma((layers, dp_size)),
        dma((layers, 2)),
    ]
    hbm = pl.BlockSpec(memory_space=pl.ANY)
    state = jax.ShapeDtypeStruct((layers * seqs * groups, states), F32)
    hidden, new_re, new_im = pl.pallas_call(
        functools.partial(kernel, tp_size, dp_size, bundle),
        out_shape=(jax.ShapeDtypeStruct((seqs, feats), BF16), state, state),
        in_specs=[hbm] * 15,
        out_specs=(pl.BlockSpec(memory_space=pltpu.VMEM), hbm, hbm),
        scratch_shapes=scratch,
        compiler_params=pltpu.CompilerParams(collective_id=0, has_side_effects=True),
    )(
        tokens,
        gain,
        w_in,
        w_gate,
        rate,
        freq,
        log_step,
        flat(map_re),
        flat(map_im),
        flat(read_re),
        flat(read_im),
        skip,
        w_out,
        rows(state_re),
        rows(state_im),
    )
    return hidden, new_re.reshape(state_re.shape), new_im.reshape(state_im.shape)


def solution(mesh):
    return jax.shard_map(
        functools.partial(local, mesh.shape["tp"], mesh.shape["dp"]),
        mesh=mesh,
        in_specs=(
            P("dp", "tp"),
            P(),
            P(None, "dp", "tp"),
            P(None, "dp", "tp"),
            P(None, "tp", None),
            P(None, "tp", None),
            P(None, "tp"),
            P(None, "tp", None, None),
            P(None, "tp", None, None),
            P(None, "tp", None, None),
            P(None, "tp", None, None),
            P(None, "tp", None),
            P(None, "dp", "tp"),
            P(None, "dp", "tp", None),
            P(None, "dp", "tp", None),
        ),
        out_specs=(P("dp", "tp"), P(None, "dp", "tp", None), P(None, "dp", "tp", None)),
        check_vma=False,
    )
```

time: 174 us -> 45 us (0.26)
  blocking collectives: 124 us -> 0 us
  Pallas kernels: 0 us -> 40.3 us
  matrix products: 15.2 us -> 0 us
  between operations: 14.5 us -> 0.65 us
  waiting for transfers between devices: 11.8 us -> 0 us
  local copies, waits for them, and re-layouts: 6.96 us -> 3.74 us
    all_gather x4 -> x0, blocking collectives: 124 us -> none  [the longest x2 62.9 us: local(): whole = lax.all_gather(hidden, 'tp', axis=1, tiled=True)]
    pallas_call x0 -> x1, Pallas kernels: none -> 40.3 us  [local(): pl.pallas_call(functools.partial(kernel, tp_size, dp_size, bundle), out_s...]
    dot_general x14 -> x0, matrix products: 15.2 us -> none  [the longest x2 4.87 us: local(): jnp.dot(full_rows, lax.all_gather(w_out[layer], 'dp', axis=0, tiled=True)...]
    all_gather x6 -> x0, waiting for transfers between devices: 10.2 us -> none  [the longest x2 10.2 us: local(): lax.all_gather(w_gate[layer], 'dp', axis=0, tiled=True)]
    slice x5 -> x0, local copies, waits for them, and re-layouts: 4.5 us -> none  [the longest x1 2.35 us: local(): w_in[layer]]
    unnamed x30 -> x5, local copies, waits for them, and re-layouts: 1.92 us -> 3.74 us
  transfers between devices with their start and end apart: 6 -> 0, of which waited for: 2 -> 0; matrix products, arithmetic and copies ran while one was open for 10% -> 0% of each run, Pallas kernels for 0% -> 0%
where the time goes in v1:
time: 45 us; the launch traced here: 44.7 us
  Pallas kernels  40.3 us (90%)
  local copies, waits for them, and re-layouts  3.74 us (8%)
  between operations  0.65 us (1%)
    pallas_call x1, Pallas kernels, local(): pl.pallas_call(functools.partial(kernel, tp_size, dp_size, bundle), out_s...  40.3 us
    unnamed x5, local copies, waits for them, and re-layouts  3.74 us

profile of v1, /device:TPU:0, one launch (start us, length us, event | category | flops | bytes accessed | tf_op | source)
XLA Modules:
  0.0 44.7 jit_solution(7598848172652255760)
XLA Ops:
  0.6 40.3 %shard_map.166 = (bf16[16,512]{1,0:T(8,128)(2,1)}, f32[512,64]{1,0:T(8,128)}, f32[512,64]{1,0:T(8,128)}) custom-call(bf16[16,512]{1,0:T(8,128)(2,1)} %tokens.1, f32[2,4096]{1,0:T(2,128)} %gain.1, bf16[2,1024,256]{2,1,0:T(8,128)(2,1)} %w_in.1, bf16[2,1024,256]{2,1,0:T(8,128)(2,1)} %w_gate.1, f32[2,16,64]{2,1,0:T(8,128)} %rate.1, f32[2,16,64]{2,1,0:T(8,128)} %freq.1, ...), custom_call_target="tpu_custom_call" | custom-call | tf_op jit(solution)/shard_map/pallas_call | solution.py:381
  40.9 1.3 %copy.21 = bf16[16,512]{1,0:T(8,128)(2,1)} copy(bf16[16,512]{1,0:T(8,128)(2,1)} %get-tuple-element.12) | data formatting | bytes 32768
  42.3 0.0 copy-start
  42.3 1.7 %copy.22 = f32[2,16,16,64]{3,2,1,0:T(8,128)} copy(f32[2,16,16,64]{3,2,1,0:T(8,128)} %bitcast.9) | data formatting | bytes 262144
  44.0 0.0 copy-done
  44.0 0.7 %copy.23 = f32[2,16,16,64]{3,2,1,0:T(8,128)} copy(f32[2,16,16,64]{3,2,1,0:T(8,128)S(1)} %bitcast.8) | data formatting | bytes 262144
Async XLA Ops:
  42.3 1.7 %copy-start = (f32[512,64]{1,0:T(8,128)S(1)}, f32[512,64]{1,0:T(8,128)}, u32[]{:S(2)}) copy-start(f32[512,64]{1,0:T(8,128)} %get-tuple-element.8) | copy-start | bytes 393220

commit v2 on v1

--- a/solution.py
+++ b/solution.py
@@ -98,6 +98,20 @@
     slot = lax.rem(j, per)
     is_self = target == i
 
+    barrier = pltpu.get_barrier_semaphore()
+    for t in range(per):
+        for d in range(dp_size):
+            src_tp = i * per + t
+
+            @pl.when(jnp.logical_or(src_tp != j, i != d))
+            def _():
+                pl.semaphore_signal(barrier, inc=1, device_id={"tp": src_tp, "dp": jnp.int32(d)})
+
+    for r in range(1, dp_size):
+        pl.semaphore_signal(
+            barrier, inc=1, device_id={"tp": j, "dp": lax.rem(i + r, dp_size)}
+        )
+
     gain_cols = pl.ds(pl.multiple_of(i * depth, depth), depth)
     loads = [
         (tokens, tok),
@@ -122,22 +136,8 @@
     for copy in copies:
         copy.start()
 
-    barrier = pltpu.get_barrier_semaphore()
-    for t in range(per):
-        for d in range(dp_size):
-            src_tp = i * per + t
-
-            @pl.when(jnp.logical_or(src_tp != j, i != d))
-            def _():
-                pl.semaphore_signal(barrier, inc=1, device_id={"tp": src_tp, "dp": jnp.int32(d)})
-
-    for r in range(1, dp_size):
-        pl.semaphore_signal(
-            barrier, inc=1, device_id={"tp": j, "dp": lax.rem(i + r, dp_size)}
-        )
-
     pending = []
-    order = sorted(range(tp_size), key=lambda r: -min(r, tp_size - r))
+    order = list(range(tp_size))
 
     def spread(src, buf, send, recv, layer):
         dst = buf.at[layer, slot, i]
@@ -317,6 +317,20 @@
         else:
             copy.wait_send()
     for copy in out_copies:
+        copy.wait()
+
+
+def finish(*refs):
+    n = 3
+    ins, outs, bufs, sem_in, sem_out = refs[:n], refs[n : 2 * n], refs[2 * n : 3 * n], refs[-2], refs[-1]
+    reads = [pltpu.make_async_copy(a, b, sem_in.at[k]) for k, (a, b) in enumerate(zip(ins, bufs))]
+    writes = [pltpu.make_async_copy(a, b, sem_out.at[k]) for k, (a, b) in enumerate(zip(bufs, outs))]
+    for copy in reads:
+        copy.start()
+    for a, b in zip(reads, writes):
+        a.wait()
+        b.start()
+    for copy in writes:
         copy.wait()
 
 
@@ -402,6 +416,13 @@
         rows(state_re),
         rows(state_im),
     )
+    hidden, new_re, new_im = pl.pallas_call(
+        finish,
+        out_shape=(jax.ShapeDtypeStruct((seqs, feats), BF16), state, state),
+        in_specs=[hbm] * 3,
+        out_specs=[hbm] * 3,
+        scratch_shapes=[vm((seqs, feats), BF16), vm(state.shape, F32), vm(state.shape, F32), dma((3,)), dma((3,))],
+    )(hidden, new_re, new_im)
     return hidden, new_re.reshape(state_re.shape), new_im.reshape(state_im.shape)
 
 

time: 45 us -> 42.4 us (0.942)
  local copies, waits for them, and re-layouts: 3.74 us -> 0 us
  Pallas kernels: 40.3 us -> 41.4 us
    unnamed x5 -> x0, local copies, waits for them, and re-layouts: 3.74 us -> none
    pallas_call x0 -> x1, Pallas kernels: none -> 1.81 us  [local(): pl.pallas_call(finish, out_shape=(jax.ShapeDtypeStruct((seqs, feats), BF1...]
    pallas_call x1, Pallas kernels: 40.3 us -> 39.6 us  [local(): pl.pallas_call(functools.partial(kernel, tp_size, dp_size, bundle), out_s...]
where the time goes in v2:
time: 42.4 us; the launch traced here: 42 us
  Pallas kernels  41.4 us (98%)
  between operations  0.64 us (2%)
    pallas_call x1, Pallas kernels, local(): pl.pallas_call(functools.partial(kernel, tp_size, dp_size, bundle), out_s...  39.6 us
    pallas_call x1, Pallas kernels, local(): pl.pallas_call(finish, out_shape=(jax.ShapeDtypeStruct((seqs, feats), BF1...  1.81 us

profile of v2, /device:TPU:0, one launch (start us, length us, event | category | flops | bytes accessed | tf_op | source)
XLA Modules:
  0.0 42.0 jit_solution(16905021999178960008)
XLA Ops:
  0.6 39.6 %shard_map.166 = (bf16[16,512]{1,0:T(8,128)(2,1)}, f32[512,64]{1,0:T(8,128)}, f32[512,64]{1,0:T(8,128)}) custom-call(bf16[16,512]{1,0:T(8,128)(2,1)} %tokens.1, f32[2,4096]{1,0:T(2,128)} %gain.1, bf16[2,1024,256]{2,1,0:T(8,128)(2,1)} %w_in.1, bf16[2,1024,256]{2,1,0:T(8,128)(2,1)} %w_gate.1, f32[2,16,64]{2,1,0:T(8,128)} %rate.1, f32[2,16,64]{2,1,0:T(8,128)} %freq.1, ...), custom_call_target="tpu_custom_call" | custom-call | tf_op jit(solution)/shard_map/pallas_call | solution.py:395
  40.2 1.8 %shard_map.167 = (bf16[16,512]{1,0:T(8,128)(2,1)}, f32[512,64]{1,0:T(8,128)}, f32[512,64]{1,0:T(8,128)}) custom-call(bf16[16,512]{1,0:T(8,128)(2,1)} %get-tuple-element.9.refs_0_, f32[512,64]{1,0:T(8,128)} %get-tuple-element.10.refs_1_, f32[512,64]{1,0:T(8,128)} %get-tuple-element.11.refs_2_), custom_call_target="tpu_custom_call" | custom-call | tf_op jit(solution)/shard_map/pallas_call | solution.py:419

commit v3 on v2

--- a/solution.py
+++ b/solution.py
@@ -72,6 +72,8 @@
     obuf,
     orbuf,
     hid,
+    sgate,
+    rgate,
     load_sem,
     a_send,
     a_recv,
@@ -81,6 +83,8 @@
     c_recv,
     d_send,
     d_recv,
+    e_send,
+    e_recv,
     out_sem,
 ):
     j = lax.axis_index("tp")
@@ -137,7 +141,7 @@
         copy.start()
 
     pending = []
-    order = list(range(tp_size))
+    order = list(range(tp_size))[::-1]
 
     def spread(src, buf, send, recv, layer):
         dst = buf.at[layer, slot, i]
@@ -249,29 +253,33 @@
         gather_wait(xbuf, a_recv, layer)
         squares = jnp.zeros((rows_all, 1), F32)
         drive_sum = jnp.zeros((rows_all, cols), F32)
-        gate_sum = jnp.zeros((rows_all, cols), F32)
+        operands = []
         for t in range(per):
             part = slice(t * feats, (t + 1) * feats)
             x = xbuf[layer, t].reshape(rows_all, feats).astype(F32)
             squares = squares + jnp.sum(x * x, axis=1, keepdims=True)
             scaled = (x * gain_v[layer : layer + 1, part]).astype(BF16)
             drive_sum = drive_sum + dot(scaled, win_v[layer, part, :])
-            gate_sum = gate_sum + dot(scaled, wgate_v[layer, part, :])
+            operands.append(scaled)
         high = squares.astype(BF16).astype(F32)
         lane = lax.broadcasted_iota(jnp.int32, (rows_all, TAIL), 1)
         tail = jnp.where(lane < TAIL // 2, high, squares - high).astype(BF16)
         sbuf[layer, :, :, 0:TAIL] = tail.reshape(dp_size, seqs, TAIL)
-        sbuf[layer, :, :, TAIL : TAIL + cols] = drive_sum.astype(BF16).reshape(
+        sbuf[layer, :, :, TAIL:] = drive_sum.astype(BF16).reshape(
             dp_size, seqs, cols
         )
-        sbuf[layer, :, :, TAIL + cols :] = gate_sum.astype(BF16).reshape(dp_size, seqs, cols)
         scatter(sbuf, rbuf, b_send, b_recv, layer)
+        gate_sum = jnp.zeros((rows_all, cols), F32)
+        for t in range(per):
+            part = slice(t * feats, (t + 1) * feats)
+            gate_sum = gate_sum + dot(operands[t], wgate_v[layer, part, :])
+        sgate[layer] = gate_sum.astype(BF16).reshape(dp_size, seqs, cols)
+        scatter(sgate, rgate, e_send, e_recv, layer)
         acc = collect(sbuf, rbuf, b_recv, layer)
         mean = (acc[:, 0:1] + acc[:, TAIL // 2 : TAIL // 2 + 1]) * (1.0 / total_feats)
         inv_scale = lax.rsqrt(mean + EPSILON)
-        projected = (acc[:, TAIL : TAIL + cols] * inv_scale).astype(BF16)
-        gate = (acc[:, TAIL + cols :] * inv_scale).astype(BF16).astype(F32)
-        fresh = []
+        projected = (acc[:, TAIL:] * inv_scale).astype(BF16)
+        fresh, lit = [], []
         for q in range(bundles):
             part = slice(q * bc, (q + 1) * bc)
             u = projected[:, part]
@@ -280,9 +288,13 @@
             readout = dot_t(new.astype(BF16), read[layer, q])
             readout = readout + skip_flat[layer, 0:1, part] * u.astype(F32)
             inner = 0.7978845608028654 * (readout + 0.044715 * readout * readout * readout)
-            activated = 0.5 * readout * (1.0 + jnp.tanh(inner))
+            lit.append(0.5 * readout * (1.0 + jnp.tanh(inner)))
+        gate = collect(sgate, rgate, e_recv, layer) * inv_scale
+        gate = gate.astype(BF16).astype(F32)
+        for q in range(bundles):
+            part = slice(q * bc, (q + 1) * bc)
             opened = 0.5 * (jnp.tanh(0.5 * gate[:, part]) + 1.0)
-            mix[layer, :, part] = (activated * opened).astype(BF16)
+            mix[layer, :, part] = (lit[q] * opened).astype(BF16)
         spread(mix.at[layer], mbuf, c_send, c_recv, layer)
         for g in range(groups):
             q, k = g // bundle, g % bundle
@@ -346,7 +358,7 @@
     bc, bn = bundle * channels, bundle * states
     flat = lambda a: a.reshape(layers, groups * channels, states)
     rows = lambda a: a.reshape(layers * seqs * groups, states)
-    width = TAIL + 2 * cols
+    width = TAIL + cols
     vm = pltpu.VMEM
     dma = pltpu.SemaphoreType.DMA
     scratch = [
@@ -379,6 +391,8 @@
         vm((layers, dp_size, seqs, feats), BF16),
         vm((layers, dp_size, seqs, feats), BF16),
         vm((layers, seqs, feats), BF16),
+        vm((layers, dp_size, seqs, cols), BF16),
+        vm((layers, dp_size, seqs, cols), BF16),
         dma((15,)),
         dma((layers, tp_size)),
         dma((layers, per, dp_size)),
@@ -386,6 +400,8 @@
         dma((layers, dp_size)),
         dma((layers, tp_size)),
         dma((layers, per, dp_size)),
+        dma((layers, dp_size)),
+        dma((layers, dp_size)),
         dma((layers, dp_size)),
         dma((layers, dp_size)),
         dma((layers, 2)),

time: 42.4 us -> 41.9 us (0.988)
  no operation moved by 1% of the time
where the time goes in v3:
time: 41.9 us; the launch traced here: 41.6 us
  Pallas kernels  41 us (98%)
  between operations  0.64 us (2%)
    pallas_call x1, Pallas kernels, local(): pl.pallas_call(functools.partial(kernel, tp_size, dp_size, bundle), out_s...  39.1 us
    pallas_call x1, Pallas kernels, local(): pl.pallas_call(finish, out_shape=(jax.ShapeDtypeStruct((seqs, feats), BF1...  1.81 us

profile of v3, /device:TPU:0, one launch (start us, length us, event | category | flops | bytes accessed | tf_op | source)
XLA Modules:
  0.0 41.6 jit_solution(14671193472302461234)
XLA Ops:
  0.6 39.1 %shard_map.166 = (bf16[16,512]{1,0:T(8,128)(2,1)}, f32[512,64]{1,0:T(8,128)}, f32[512,64]{1,0:T(8,128)}) custom-call(bf16[16,512]{1,0:T(8,128)(2,1)} %tokens.1, f32[2,4096]{1,0:T(2,128)} %gain.1, bf16[2,1024,256]{2,1,0:T(8,128)(2,1)} %w_in.1, bf16[2,1024,256]{2,1,0:T(8,128)(2,1)} %w_gate.1, f32[2,16,64]{2,1,0:T(8,128)} %rate.1, f32[2,16,64]{2,1,0:T(8,128)} %freq.1, ...), custom_call_target="tpu_custom_call" | custom-call | tf_op jit(solution)/shard_map/pallas_call | solution.py:411
  39.8 1.8 %shard_map.167 = (bf16[16,512]{1,0:T(8,128)(2,1)}, f32[512,64]{1,0:T(8,128)}, f32[512,64]{1,0:T(8,128)}) custom-call(bf16[16,512]{1,0:T(8,128)(2,1)} %get-tuple-element.9.refs_0_, f32[512,64]{1,0:T(8,128)} %get-tuple-element.10.refs_1_, f32[512,64]{1,0:T(8,128)} %get-tuple-element.11.refs_2_), custom_call_target="tpu_custom_call" | custom-call | tf_op jit(solution)/shard_map/pallas_call | solution.py:435
